TPU v7x, 128 devices: a whole 4x4x4 slice. The times are simulated.
128 devices in a mesh: sp: 32 (over y, x, core), tp: 4 (over z).
Axes of the slice: x: 4, y: 4, z: 4, core: 2. Of those that a mesh axis runs over, the one named last changes fastest.
Arguments:
- block_input: bfloat16 [4096, 1024], P('sp'), may hold values from -6 to 6
- w_query: bfloat16 [1024, 1024], P(None, 'tp'), may hold values from -0.1875 to 0.1875
- w_forget_fwd: bfloat16 [1024, 1024], P(None, 'tp'), may hold values from -0.1875 to 0.1875
- w_forget_bwd: bfloat16 [1024, 1024], P(None, 'tp'), may hold values from -0.1875 to 0.1875
- w_value: bfloat16 [1024, 1024], P(None, 'tp'), may hold values from -0.1875 to 0.1875
- floor_rate: float32 [2, 1024], P(None, 'tp'), may hold values from 0.2 to 6
- gain: float32 [128], replicated, may hold values from 0.1 to 1.9
- cotangent: bfloat16 [4096, 1024], P('sp', 'tp'), may hold values from -6 to 6
Outputs:
- grad_input: bfloat16 [4096, 1024], P(('sp', 'tp'))
- grad_query_weight: float32 [1024, 1024], P('sp', 'tp')
- grad_floor: float32 [2, 1024], P(None, 'tp')
All inputs are finite; a program needn't handle non-finite values.
Results may differ from a plain program's by a relative error of at most 0.0045.
Values sent between devices are 32-bit elements.
No kernel may reach another device: no remote copies, remote signals or barrier semaphores. Data moves between devices by JAX's collectives and lax.ppermute only.
A program may use at most 64 MiB of HBM per device.

v0:
```python
import jax
import jax.numpy as jnp
from jax import lax
from jax.experimental import pallas as pl
from jax.experimental.pallas import tpu as pltpu
from jax.sharding import Mesh
from jax.sharding import PartitionSpec as P


SP = ("sp_0", "sp_1", "sp_2")
SP_TP = ("sp_0", "sp_1", "sp_2", "tp")
N = 32
T = 128
K = 128
HEADS = 2
W = HEADS * K
D = 1024
TOKENS = 4096.0
Q_SCALE = K ** (-0.5)
OUT_SCALE = TOKENS ** (-0.5)
NORM_EPS = 1e-06
F32 = jnp.float32
BF16 = jnp.bfloat16
NN = ((1,), (0,))
NT = ((1,), (1,))
VMEM = pl.BlockSpec(memory_space=pltpu.VMEM)
SMEM = pl.BlockSpec(memory_space=pltpu.SMEM)
HBM = pl.BlockSpec(memory_space=pltpu.HBM)
VMEM_LIMIT = 8 << 20
PROJECT_LIMIT = 67043328 - (900 << 10)
MANY, FEW = 400_000_000, 10_000_000


def dot(a, b, dims):
    return lax.dot_general(a, b, (dims, ((), ())), preferred_element_type=F32)


def split(a):
    high = a.astype(BF16)
    return high, (a - high.astype(F32)).astype(BF16)


def dot3(a, b, dims):
    (ah, al), (bh, bl) = split(a), split(b)
    return dot(ah, bh, dims) + (dot(ah, bl, dims) + dot(al, bh, dims))


def dot2(a, b, dims):
    bh, bl = split(b)
    return dot(a, bh, dims) + dot(a, bl, dims)


def dot2r(a, b, dims):
    ah, al = split(a)
    return dot(ah, b, dims) + dot(al, b, dims)


def lower_triangle():
    row = lax.broadcasted_iota(jnp.int32, (T, T), 0)
    col = lax.broadcasted_iota(jnp.int32, (T, T), 1)
    return row >= col, row <= col


def opening_of(rate):
    r = rate * (1.0 / TOKENS)
    return r * (1.0 - r * (1 / 2) * (1.0 - r * (1 / 3) * (1.0 - r * (1 / 4))))


def gates(raw, opening):
    x = raw.astype(F32)
    closed = 1.0 / (1.0 + jnp.exp(x))
    return closed, opening * closed


def log_forget_of(key):
    return -key * (1.0 + key * (1 / 2 + key * (1 / 3 + key * (1 / 4 + key * (1 / 5)))))


def fetch(sources, buffers, sems):
    def one(i):
        copy = pltpu.make_async_copy(sources[i], buffers[i], sems.at[i])
        copy.start()

        def value():
            copy.wait()
            return buffers[i][...]

        return value

    return [one(i) for i in range(len(sources))]


def project_kernel(
    x_hbm, wf_hbm, wb_hbm, wv_hbm, rate_hbm, f_ref, b_ref, v_ref, cf_ref, cb_ref, msg_ref, x_buf, w_buf, rate_buf, sems
):
    get_x, get_wf, get_rate, get_wb, get_wv = fetch(
        (x_hbm, wf_hbm, rate_hbm, wb_hbm, wv_hbm), (x_buf, w_buf.at[0], rate_buf, w_buf.at[1], w_buf.at[2]), sems
    )
    x = get_x()
    low, up = lower_triangle()
    low, up = low.astype(BF16), up.astype(BF16)
    opening = opening_of(get_rate())
    decayed = []
    for d, (get_w, raw_ref, cum_ref, tri) in enumerate(((get_wf, f_ref, cf_ref, low), (get_wb, b_ref, cb_ref, up))):
        raw = dot(x, get_w(), NN).astype(BF16)
        raw_ref[...] = raw
        _, key = gates(raw, opening[d : d + 1])
        cum = dot2(tri, log_forget_of(key), NN)
        cum_ref[...] = cum
        last = cum[T - 1 : T] if d == 0 else cum[0:1]
        decayed.append((jnp.exp(last), key * jnp.exp(last - cum)))
    v = dot(x, get_wv(), NN).astype(BF16)
    v_ref[...] = v
    for h in range(HEADS):
        cols = slice(h * K, (h + 1) * K)
        v_t = v[:, cols].astype(F32).T.astype(BF16)
        group = slice(h * 16, (h + 1) * 16)
        msg_ref[group, 16:24, :] = jnp.zeros((16, 8, K), F32)
        both = dot2(v_t, jnp.concatenate([left[:, cols] for _, left in decayed], axis=1), NN)
        for d, (all_keep, left) in enumerate(decayed):
            msg_ref[group, 8 * d : 8 * d + 8, :] = both[:, d * K : (d + 1) * K].reshape(16, 8, K)
            msg_ref[group, 16 + d : 17 + d, :] = jnp.broadcast_to(all_keep[:, cols].reshape(1, 1, K), (16, 1, K))


def local_kernel(
    x_hbm, wq_hbm, f_ref, b_ref, v_ref, cf_ref, cb_ref, rate_ref, gain_ref, cot_ref,
    a_ref, scores_ref, inner_ref, reach_ref, tail_ref, share_ref, scaled_ref, x_buf, w_buf, sems,
):
    get_x, get_wq = fetch((x_hbm, wq_hbm), (x_buf, w_buf), sems)
    low, up = lower_triangle()
    opening = opening_of(rate_ref[...])
    query = dot(get_x(), get_wq(), NN).astype(BF16).astype(F32) * Q_SCALE
    for h in range(HEADS):
        cols = slice(h * K, (h + 1) * K)
        v = v_ref[:, cols]
        v_t = v.astype(F32).T.astype(BF16)
        scores = jnp.zeros((T, T), F32)
        zs = []
        for d, (raw_ref, cum_ref, tri) in enumerate(((f_ref, cf_ref, low), (b_ref, cb_ref, up))):
            closed, key = gates(raw_ref[:, cols], opening[d : d + 1, cols])
            cum = cum_ref[:, cols]
            fade = jnp.exp(-cum)
            last = cum[T - 1 : T] if d == 0 else cum[0:1]
            a = query[:, cols] * jnp.exp(cum)
            b = key * fade
            both = slice((2 * h + d) * K, (2 * h + d + 1) * K)
            a_ref[:, both] = a
            scores = scores + jnp.where(tri, dot3(a, b, NT), 0.0)
            share = closed / (1.0 - key)
            before = dot2(tri.astype(BF16), share, NN)
            share_ref[:, both] = before
            total = before[T - 1 : T] if d == 0 else before[0:1]
            keep = jnp.exp(last)
            zs.append(keep * fade * (closed - (total - before) * key))
            tail_ref[2 * h + d : 2 * h + d + 1, :] = keep * total
        scores_ref[:, cols] = scores
        scaled_ref[:, cols] = cot_ref[:, cols].astype(F32) * gain_ref[...]
        inner_ref[:, cols] = dot2r(scores, v, NN)
        reach_ref[:, 2 * h * K : 2 * (h + 1) * K] = dot2(v_t, jnp.concatenate(zs, axis=1), NN)


def scan_kernel(got_ref, out_ref, keep_ref):
    keep_ref[...] = got_ref[:, 16:24, :]
    run_f = run_b = jnp.zeros((8, K), F32)
    for i in range(N):
        j = N - 1 - i
        out_ref[i, 0:8, :] = run_f
        out_ref[j, 8:16, :] = run_b
        run_f = got_ref[i, 16:17, :] * run_f + got_ref[i, 0:8, :]
        run_b = got_ref[j, 17:18, :] * run_b + got_ref[j, 8:16, :]


def states_of(ref, h):
    group = slice(h * 16, (h + 1) * 16)
    return [ref[group, 8 * d : 8 * d + 8, :].reshape(K, K) for d in range(2)]


def mix_kernel(a_ref, inner_ref, reach_ref, tail_ref, scaled_ref, in_ref, msg_ref, dm_ref):
    for h in range(HEADS):
        cols = slice(h * K, (h + 1) * K)
        wide = slice(2 * h * K, 2 * (h + 1) * K)
        group = slice(h * 16, (h + 1) * 16)
        a = a_ref[:, wide]
        states = jnp.concatenate(states_of(in_ref, h), axis=1)
        mixed = inner_ref[:, cols] + dot3(a, states, NT)
        inv = lax.rsqrt(jnp.mean(mixed * mixed, axis=-1, keepdims=True) + NORM_EPS)
        scaled = scaled_ref[:, cols]
        d_mixed = inv * scaled - mixed * (inv * inv * inv * jnp.mean(scaled * mixed, axis=-1, keepdims=True))
        dm_ref[:, cols] = d_mixed
        seeds = dot3(d_mixed.T, a, NN)
        tail = jnp.concatenate([tail_ref[2 * h + d : 2 * h + d + 1, :] for d in range(2)], axis=1)
        reach = reach_ref[:, wide] - tail * states
        for d in range(2):
            half = slice(d * K, (d + 1) * K)
            msg_ref[group, 8 * d : 8 * d + 8, :] = seeds[:, half].reshape(16, 8, K)
            msg_ref[group, 16 + 8 * d : 24 + 8 * d, :] = reach[:, half].reshape(16, 8, K)


def query_kernel(
    core_ref, x_hbm, f_ref, b_ref, cf_ref, cb_ref, rate_ref, v_ref, a_ref, in_ref, dm_ref,
    own_ref, other_ref, gq_ref, local_ref, ada_ref, x_buf, sems,
):
    (get_x,) = fetch((x_hbm,), (x_buf,), sems)
    low, up = lower_triangle()
    opening = opening_of(rate_ref[...])
    grad_q = []
    for h in range(HEADS):
        cols = slice(h * K, (h + 1) * K)
        d_mixed = dm_ref[:, cols]
        d_scores = dot2r(d_mixed, v_ref[:, cols], NT)
        dq = jnp.zeros((T, K), F32)
        for d, (state, raw_ref, cum_ref, tri) in enumerate(
            zip(states_of(in_ref, h), (f_ref, b_ref), (cf_ref, cb_ref), (low, up))
        ):
            _, key = gates(raw_ref[:, cols], opening[d : d + 1, cols])
            cum = cum_ref[:, cols]
            both = slice((2 * h + d) * K, (2 * h + d + 1) * K)
            local = jnp.where(tri, d_scores, 0.0)
            local_ref[:, both] = local
            da = dot3(
                jnp.concatenate([local, d_mixed], axis=1), jnp.concatenate([key * jnp.exp(-cum), state], axis=0), NN
            )
            dq = dq + da * jnp.exp(cum)
            ada_ref[:, both] = a_ref[:, both] * da
        grad_q.append((dq * Q_SCALE).astype(BF16))
    gq = jnp.concatenate(grad_q, axis=1)
    gq_ref[...] = gq
    term = dot(get_x().astype(F32).T.astype(BF16), gq, NN).reshape(N, 2, 16, W)
    first = core_ref[0] == 0
    own = jnp.where(first, term[:, 0], term[:, 1])
    other = jnp.where(first, term[:, 1], term[:, 0])
    for part, ref in ((own, own_ref), (other, other_ref)):
        for h in range(HEADS):
            ref[:, 16 * h : 16 * h + 16, :] = part[:, :, h * K : (h + 1) * K]


def key_kernel(
    f_ref, b_ref, cf_ref, cb_ref, rate_ref, a_ref, scores_ref, share_ref, local_ref, ada_ref, dm_ref,
    db_ref, dv_ref, floor_ref,
):
    opening = opening_of(rate_ref[...])
    for h in range(HEADS):
        cols = slice(h * K, (h + 1) * K)
        dv_ref[:, cols] = dot3(scores_ref[:, cols].T, dm_ref[:, cols], NN)
        for d, (raw_ref, cum_ref) in enumerate(((f_ref, cf_ref), (b_ref, cb_ref))):
            both = slice((2 * h + d) * K, (2 * h + d + 1) * K)
            db = dot3(local_ref[:, both].T, a_ref[:, both], NN)
            db_ref[:, both] = db
            closed, key = gates(raw_ref[:, cols], opening[d : d + 1, cols])
            faded = db * jnp.exp(-cum_ref[:, cols])
            floor = closed * faded - share_ref[:, both] * (ada_ref[:, both] - key * faded)
            floor_ref[2 * h + d : 2 * h + d + 1, :] = jnp.sum(floor, axis=0, keepdims=True)


def scan_back_kernel(keep_ref, got_ref, own_ref, other_ref, local_ref, out_ref):
    run_f = run_b = reach_f = reach_b = jnp.zeros((8, K), F32)
    for i in range(N):
        j = N - 1 - i
        out_ref[j, 0:8, :] = run_f
        out_ref[i, 8:16, :] = run_b
        reach_f = reach_f + run_f * got_ref[j, 16:24, :]
        reach_b = reach_b + run_b * got_ref[i, 24:32, :]
        run_f = keep_ref[j, 0:1, :] * run_f + got_ref[j, 0:8, :]
        run_b = keep_ref[i, 1:2, :] * run_b + got_ref[i, 8:16, :]
    out_ref[:, 16:48, :] = own_ref[...] + other_ref[...]
    tail = [jnp.sum(reach_f, axis=0, keepdims=True), jnp.sum(reach_b, axis=0, keepdims=True)]
    tail = jnp.concatenate(tail + [local_ref[...], jnp.zeros((2, K), F32)], axis=0)
    out_ref[:, 48:56, :] = jnp.broadcast_to(tail[None], (N, 8, K))


def finish_kernel(
    f_ref, b_ref, v_ref, cf_ref, cb_ref, rate_ref, in_ref, got_ref,
    db_ref, dv_ref, ada_ref, gq_ref, wq_hbm, wf_hbm, wb_hbm, wv_hbm,
    term_ref, weight_ref, floor_ref, w_buf, sems,
):
    weights = fetch((wq_hbm, wf_hbm, wb_hbm, wv_hbm), [w_buf.at[i] for i in range(4)], sems)
    low, up = lower_triangle()
    rate = rate_ref[...]
    opening = opening_of(rate)
    g_raw = ([], [])
    g_value = []
    rows = got_ref[:, 48:56, :]
    local_floor = jnp.sum(rows, axis=0)
    floors = ([], [])
    for h in range(HEADS):
        cols = slice(h * K, (h + 1) * K)
        flows = states_of(got_ref, h)
        flow = jnp.concatenate(flows, axis=1)
        states = states_of(in_ref, h)
        d_lefts = dot2(v_ref[:, cols], flow, NN)
        owned = jnp.sum(rows[h * 16 : (h + 1) * 16], axis=0)
        lefts = []
        for d, (raw_ref, cum_ref, rev) in enumerate(((f_ref, cf_ref, up), (b_ref, cb_ref, low))):
            both = slice((2 * h + d) * K, (2 * h + d + 1) * K)
            _, key = gates(raw_ref[:, cols], opening[d : d + 1, cols])
            opened = 1.0 / (1.0 + jnp.exp(-raw_ref[:, cols].astype(F32)))
            cum = cum_ref[:, cols]
            last = cum[T - 1 : T] if d == 0 else cum[0:1]
            keep = jnp.exp(last)
            fade = jnp.exp(-cum)
            b = key * fade
            left = b * keep
            lefts.append(left)
            d_left = d_lefts[:, d * K : (d + 1) * K]
            db = db_ref[:, both] + keep * d_left
            dc = ada_ref[:, both] - b * db
            total = jnp.sum(left * d_left, axis=0, keepdims=True)
            total = total + keep * jnp.sum(states[d] * flows[d], axis=0, keepdims=True)
            d_log = dot2(rev.astype(BF16), dc, NN) + total
            whole = db * fade - d_log / (1.0 - key)
            g_raw[d].append((-key * opened * whole).astype(BF16))
            floors[d].append(owned[d : d + 1] + local_floor[2 + 2 * h + d : 3 + 2 * h + d])
        dv = dv_ref[:, cols] + dot3(jnp.concatenate(lefts, axis=1), flow, NT)
        g_value.append(dv.astype(BF16))
    parts = [gq_ref[...]] + [jnp.concatenate(part, axis=1) for part in (g_raw[0], g_raw[1], g_value)]
    out = dot(parts[0], weights[0](), NT)
    for part, get_w in zip(parts[1:], weights[1:]):
        out = out + dot(part, get_w(), NT)
    term_ref[...] = out
    for c in range(2):
        acc = got_ref[c, 16:48, :]
        for j in range(1, N // 2):
            acc = acc + got_ref[2 * j + c, 16:48, :]
        for h in range(HEADS):
            weight_ref[16 * c : 16 * c + 16, h * K : (h + 1) * K] = acc[16 * h : 16 * h + 16] * OUT_SCALE
    shift = jnp.exp(rate * (-1.0 / TOKENS)) * (OUT_SCALE / TOKENS)
    for d in range(2):
        floor_ref[d : d + 1, :] = jnp.concatenate(floors[d], axis=1) * shift[d : d + 1]


def shape(*dims, dtype=F32):
    return jax.ShapeDtypeStruct(dims, dtype)


def call(kernel, out_shape, specs, flops, scratch=(), limit=VMEM_LIMIT):
    many = isinstance(out_shape, (tuple, list))
    return pl.pallas_call(
        kernel,
        out_shape=out_shape,
        in_specs=specs,
        out_specs=[VMEM] * len(out_shape) if many else VMEM,
        scratch_shapes=list(scratch),
        cost_estimate=pl.CostEstimate(flops=flops, bytes_accessed=1 << 20, transcendentals=0),
        compiler_params=pltpu.CompilerParams(vmem_limit_bytes=limit),
    )


def exchange(array, axes):
    return lax.all_to_all(array, axes, 0, 0, tiled=True)


def body(x, w_query, w_forget_fwd, w_forget_bwd, w_value, floor_rate, gain, cotangent):
    tok, wide = shape(T, W), shape(T, 2 * W)
    tok16 = shape(T, W, dtype=BF16)
    x_buf, w_buf = pltpu.VMEM((T, D), BF16), pltpu.VMEM((D, W), BF16)
    dma = pltpu.SemaphoreType.DMA
    f, b, v, cf, cb, sums = call(
        project_kernel, (tok16, tok16, tok16, tok, tok, shape(N, 24, K)), [HBM] * 5, MANY,
        (x_buf, pltpu.VMEM((3, D, W), BF16), pltpu.VMEM((2, W), F32), dma((5,))), PROJECT_LIMIT,
    )(x, w_forget_fwd, w_forget_bwd, w_value, floor_rate)
    sums = exchange(sums, SP)
    a, scores, inner, reach, tail, share, scaled = call(
        local_kernel, (wide, tok, tok, wide, shape(4, K), wide, tok), [HBM] * 2 + [VMEM] * 8, MANY,
        (x_buf, w_buf, dma((2,))),
    )(x, w_query, f, b, v, cf, cb, floor_rate, gain.reshape(1, K), cotangent)
    inflow, keeps = call(scan_kernel, (shape(N, 16, K), shape(N, 8, K)), [VMEM], FEW)(sums)
    inflow = exchange(inflow, SP)
    seeds, dm = call(mix_kernel, (shape(N, 32, K), tok), [VMEM] * 6, MANY)(
        a, inner, reach, tail, scaled, inflow
    )
    seeds = exchange(seeds, SP)
    core = lax.axis_index("sp_2").reshape(1).astype(jnp.int32)
    own, other, gq, local, ada = call(
        query_kernel, (shape(N, 32, K), shape(N, 32, K), tok16, wide, wide), [SMEM, HBM] + [VMEM] * 9,
        MANY, (x_buf, dma((1,))),
    )(core, x, f, b, cf, cb, floor_rate, v, a, inflow, dm)
    other = lax.ppermute(other, "sp_2", [(0, 1), (1, 0)])
    db, dv, floor = call(key_kernel, (wide, tok, shape(4, K)), [VMEM] * 11, MANY)(
        f, b, cf, cb, floor_rate, a, scores, share, local, ada, dm
    )
    outflow = exchange(call(scan_back_kernel, shape(N, 56, K), [VMEM] * 5, FEW)(keeps, seeds, own, other, floor), SP)
    term, grad_weight, grad_floor = call(
        finish_kernel, (shape(T, D), shape(N, W), shape(2, W)), [VMEM] * 12 + [HBM] * 4, MANY,
        (pltpu.VMEM((4, D, W), BF16), dma((4,))),
    )(
        f, b, v, cf, cb, floor_rate, inflow, outflow, db, dv, ada, gq,
        w_query, w_forget_fwd, w_forget_bwd, w_value,
    )
    pieces = exchange(term, "tp").reshape(4, T // 4, D)
    grad_input = (pieces[0] + pieces[1] + pieces[2] + pieces[3]).astype(BF16)
    return grad_input, grad_weight, grad_floor


def solution(mesh):
    finer = Mesh(mesh.devices.reshape(4, 4, 2, mesh.shape["tp"]), ("sp_0", "sp_1", "sp_2", "tp"))
    return jax.shard_map(
        body,
        mesh=finer,
        in_specs=(
            P(SP, None),
            P(None, "tp"),
            P(None, "tp"),
            P(None, "tp"),
            P(None, "tp"),
            P(None, "tp"),
            P(),
            P(SP, "tp"),
        ),
        out_specs=(P(SP_TP, None), P(SP, "tp"), P(None, "tp")),
        check_vma=False,
    )
```

profile of v0, /device:TPU:1, one launch (start us, length us, event | category | flops | bytes accessed | tf_op | source)
XLA Modules:
  0.0 94.8 jit_solution(4277493473978121482)
XLA Ops:
  0.6 3.6 %shard_map.103 = (bf16[128,256]{1,0:T(8,128)(2,1)}, bf16[128,256]{1,0:T(8,128)(2,1)}, bf16[128,256]{1,0:T(8,128)(2,1)}, f32[128,256]{1,0:T(8,128)}, f32[128,256]{1,0:T(8,128)}, /*index=5*/f32[32,24,128]{2,1,0:T(8,128)}) custom-call(bf16[128,1024]{1,0:T(8,128)(2,1)} %x_hbm.5, bf16[1024,256]{1,0:T(8,128)(2,1)} %wf_hbm.3, bf16[1024,256]{1,0:T(8,128)(2,1)} %wb_hbm.3, ...), custom_call_target="tpu_custom_call" | custom-call | flops 400000000 | bytes 1048576 | tf_op jit(solution)/shard_map/pallas_call | solution.py:357
  4.2 0.0 copy-start.8
  4.2 0.0 copy-start.21
  4.3 0.0 copy-start.26
  4.3 18.9 %all_to_all.29.got_ref = f32[32,24,128]{2,1,0:T(8,128)S(1)} all-to-all(f32[32,24,128]{2,1,0:T(8,128)} %get-tuple-element.36), channel_id=1, replica_groups=mesh['sp_0'=4,'sp_1'=4,'sp_2'=2,'tp'=4] {'sp_0','sp_1','sp_2'}, dimensions={0} | all-to-all | bytes 786432 | tf_op jit(solution)/shard_map/all_to_all | solution.py:349
  23.1 0.8 shard_map.104
  23.9 0.0 copy-start.7
  23.9 0.6 copy-done.13
  24.5 3.8 %all-to-all-start.1 = ((f32[32,16,128]{2,1,0:T(8,128)}), f32[32,16,128]{2,1,0:T(8,128)S(1)}, u32[]{:S(2)}, u32[]{:S(2)}) async-start(f32[32,16,128]{2,1,0:T(8,128)} %get-tuple-element.37), calls=%async_computation.1 | async-start | bytes 524288 | tf_op jit(solution)/shard_map/all_to_all | solution.py:349
  28.4 0.0 copy-start.25
  28.4 0.0 copy-start.27
  28.4 0.0 copy-done.8
  28.4 0.0 copy-done.21
  28.4 0.0 copy-done.26
  28.5 0.6 copy-done.25
  29.0 1.2 %shard_map.105 = (f32[128,512]{1,0:T(8,128)S(1)}, f32[128,256]{1,0:T(8,128)S(1)}, f32[128,256]{1,0:T(8,128)S(1)}, f32[128,512]{1,0:T(8,128)S(1)}, f32[4,128]{1,0...) custom-call(bf16[128,1024]{1,0:T(8,128)(2,1)S(1)} %copy-done.8, bf16[1024,256]{1,0:T(8,128)(2,1)S(1)} %copy-done.5, ...), custom_call_target="tpu_custom_call" | custom-call | flops 400000000 | bytes 1048576 | tf_op jit(solution)/shard_map/pallas_call | solution.py:362
  30.3 0.0 copy-start.9
  30.3 0.7 copy-done.9
  30.9 0.6 copy-done.17
  31.6 5.8 %all-to-all-done.1.in_ref = f32[32,16,128]{2,1,0:T(8,128)S(1)} async-done(((f32[32,16,128]{2,1,0:T(8,128)}), f32[32,16,128]{2,1,0:T(8,128)S(1)}, u32[]{:S(2)}, u32[]{:S(2)}) %all-to-all-start.1) | async-done | bytes 262176 | tf_op jit(solution)/shard_map/all_to_all | solution.py:349
  37.3 1.5 %shard_map.106 = (f32[32,32,128]{2,1,0:T(8,128)}, f32[128,256]{1,0:T(8,128)S(1)}) custom-call(f32[128,512]{1,0:T(8,128)S(1)} %get-tuple-element.39.a_ref, f32[128,256]{1,0:T(8,128)S(1)} %get-tuple-element.40.inner_ref, f32[128,512]{1,0:T(8,128)S(1)} %get-tuple-element.41.reach_ref, f32[4,128]{1,0:T(4,128)S(1)} %get-tuple-element.42.tail_ref, ...), custom_call_target="tpu_custom_call" | custom-call | flops 400000000 | bytes 1048576 | tf_op jit(solution)/shard_map/pallas_call | solution.py:368
  38.9 1.9 %shard_map.107 = (f32[32,32,128]{2,1,0:T(8,128)S(1)}, f32[32,32,128]{2,1,0:T(8,128)}, bf16[128,256]{1,0:T(8,128)(2,1)S(1)}, f32[128,512]{1,0:T(8,128)S(1)}, f32[128,512]{1,0:T(8,128)S(1)}) custom-call(s32[1]{0:T(128)} %bitcast.1.core_ref, bf16[128,1024]{1,0:T(8,128)(2,1)S(1)} %copy-done.8, bf16[128,256]{1,0:T(8,128)(2,1)S(1)} %copy-done.6, ...), custom_call_target="tpu_custom_call" | custom-call | flops 400000000 | bytes 1048576 | tf_op jit(solution)/shard_map/pallas_call | solution.py:373
  40.8 0.7 copy-done.11
  41.5 0.6 copy-done.23
  42.1 0.1 collective-permute-start
  42.3 3.9 %all-to-all-start.2 = ((f32[32,32,128]{2,1,0:T(8,128)}), f32[32,32,128]{2,1,0:T(8,128)S(1)}, u32[]{:S(2)}, u32[]{:S(2)}) async-start(f32[32,32,128]{2,1,0:T(8,128)} %get-tuple-element.44), calls=%async_computation.2 | async-start | bytes 1048576 | tf_op jit(solution)/shard_map/all_to_all | solution.py:349
  46.2 0.9 copy-done.10
  47.1 0.9 %copy-done.12 = f32[128,512]{1,0:T(8,128)S(1)} copy-done((f32[128,512]{1,0:T(8,128)S(1)}, f32[128,512]{1,0:T(8,128)}, u32[]{:S(2)}) %copy-start.12) | copy-done | bytes 262168
  48.1 0.9 copy-done.18
  49.0 0.9 copy-done.20
  49.9 0.4 shard_map.108
  50.3 0.6 copy-done.15
  51.0 6.8 %all-to-all-done.2.got_ref = f32[32,32,128]{2,1,0:T(8,128)S(1)} async-done(((f32[32,32,128]{2,1,0:T(8,128)}), f32[32,32,128]{2,1,0:T(8,128)S(1)}, u32[]{:S(2)}, u32[]{:S(2)}) %all-to-all-start.2) | async-done | bytes 524320 | tf_op jit(solution)/shard_map/all_to_all | solution.py:349
  57.7 0.0 collective-permute-done.other_ref
  57.7 0.9 copy-done.14
  58.6 0.1 shard_map.109
  58.8 0.0 copy-start
  58.8 0.0 copy-start.1
  58.8 0.0 copy-start.2
  58.8 0.0 copy-start.16
  58.8 0.0 copy-start.22
  58.8 0.0 copy-start.24
  58.8 19.4 %all_to_all.30.got_ref = f32[32,56,128]{2,1,0:T(8,128)S(1)} all-to-all(f32[32,56,128]{2,1,0:T(8,128)S(1)} %shard_map.109), channel_id=1, replica_groups=mesh['sp_0'=4,'sp_1'=4,'sp_2'=2,'tp'=4] {'sp_0','sp_1','sp_2'}, dimensions={0} | all-to-all | bytes 1835008 | tf_op jit(solution)/shard_map/all_to_all | solution.py:349
  78.2 0.0 copy-done
  78.2 0.0 copy-done.2
  78.3 2.5 %shard_map.110 = (f32[128,1024]{1,0:T(8,128)S(1)}, f32[32,256]{1,0:T(8,128)}, f32[2,256]{1,0:T(2,128)}) custom-call(bf16[128,256]{1,0:T(8,128)(2,1)S(1)} %copy-done.6, bf16[128,256]{1,0:T(8,128)(2,1)S(1)} %copy-done.7, bf16[128,256]{1,0:T(8,128)(2,1)S(1)} %copy-done.22, f32[128,256]{1,0:T(8,128)S(1)} %copy-done.3, f32[128,256]{1,0:T(8,128)S(1)} %copy-done.4, ...), custom_call_target="tpu_custom_call" | custom-call | flops 400000000 | bytes 1048576 | tf_op jit(solution)/shard_map/pallas_call | solution.py:382
  80.7 13.4 %all_to_all.31 = f32[4,32,1024]{2,1,0:T(8,128)S(1)} all-to-all(f32[4,32,1024]{2,1,0:T(8,128)S(1)} %bitcast.5), channel_id=1, replica_groups=mesh['sp_0'=4,'sp_1'=4,'sp_2'=2,'tp'=4] {'tp'}, dimensions={0} | all-to-all | bytes 1048576 | tf_op jit(solution)/shard_map/all_to_all | solution.py:349
  94.1 0.7 fusion.1
  (26 shorter events, 0.0 us)
Async XLA Ops:
  4.2 24.1 %copy-start.8 = (bf16[128,1024]{1,0:T(8,128)(2,1)S(1)}, bf16[128,1024]{1,0:T(8,128)(2,1)}, u32[]{:S(2)}) copy-start(bf16[128,1024]{1,0:T(8,128)(2,1)} %x_hbm.5) | copy-start | bytes 786436
  4.2 24.1 %copy-start.21 = (bf16[128,256]{1,0:T(8,128)(2,1)S(1)}, bf16[128,256]{1,0:T(8,128)(2,1)}, u32[]{:S(2)}) copy-start(bf16[128,256]{1,0:T(8,128)(2,1)} %get-tuple-element.33.v_ref) | copy-start | bytes 196612
  4.3 24.1 %copy-start.26 = (bf16[128,256]{1,0:T(8,128)(2,1)S(1)}, bf16[128,256]{1,0:T(8,128)(2,1)}, u32[]{:S(2)}) copy-start(bf16[128,256]{1,0:T(8,128)(2,1)} %cot_ref.1) | copy-start | bytes 196612
  23.1 5.3 %copy-start.5 = (bf16[1024,256]{1,0:T(8,128)(2,1)S(1)}, bf16[1024,256]{1,0:T(8,128)(2,1)}, u32[]{:S(2)}) copy-start(bf16[1024,256]{1,0:T(8,128)(2,1)} %wq_hbm.3) | copy-start | bytes 1572868
  23.9 0.6 copy-start.13
  23.9 4.5 %copy-start.3 = (f32[128,256]{1,0:T(8,128)S(1)}, f32[128,256]{1,0:T(8,128)}, u32[]{:S(2)}) copy-start(f32[128,256]{1,0:T(8,128)} %get-tuple-element.34.cf_ref) | copy-start | bytes 393220
  23.9 4.5 %copy-start.4 = (f32[128,256]{1,0:T(8,128)S(1)}, f32[128,256]{1,0:T(8,128)}, u32[]{:S(2)}) copy-start(f32[128,256]{1,0:T(8,128)} %get-tuple-element.35.cb_ref) | copy-start | bytes 393220
  23.9 4.5 %copy-start.6 = (bf16[128,256]{1,0:T(8,128)(2,1)S(1)}, bf16[128,256]{1,0:T(8,128)(2,1)}, u32[]{:S(2)}) copy-start(bf16[128,256]{1,0:T(8,128)(2,1)} %get-tuple-element.31.f_ref) | copy-start | bytes 196612
  23.9 4.5 %copy-start.7 = (bf16[128,256]{1,0:T(8,128)(2,1)S(1)}, bf16[128,256]{1,0:T(8,128)(2,1)}, u32[]{:S(2)}) copy-start(bf16[128,256]{1,0:T(8,128)(2,1)} %get-tuple-element.32.b_ref) | copy-start | bytes 196612
  24.5 12.8 %all-to-all-start.1 = ((f32[32,16,128]{2,1,0:T(8,128)}), f32[32,16,128]{2,1,0:T(8,128)S(1)}, u32[]{:S(2)}, u32[]{:S(2)}) async-start(f32[32,16,128]{2,1,0:T(8,128)} %get-tuple-element.37), calls=%async_computation.1 | async-start | bytes 524288 | tf_op jit(solution)/shard_map/all_to_all | solution.py:349
  28.4 0.7 copy-start.25
  28.4 0.7 copy-start.27
  30.3 0.7 copy-start.9
  30.9 0.6 copy-start.17
  38.9 1.9 %copy-start.19 = (f32[128,256]{1,0:T(8,128)}, f32[128,256]{1,0:T(8,128)S(1)}, u32[]{:S(2)}) copy-start(f32[128,256]{1,0:T(8,128)S(1)} %get-tuple-element.45.dm_ref) | copy-start | bytes 393220
  40.8 0.7 copy-start.11
  41.5 0.6 copy-start.23
  42.1 15.6 %collective-permute-start = (f32[32,32,128]{2,1,0:T(8,128)}, f32[32,32,128]{2,1,0:T(8,128)S(1)}, u32[]{:S(2)}, u32[]{:S(2)}) collective-permute-start(f32[32,32,128]{2,1,0:T(8,128)} %get-tuple-element.47), channel_id=1, source_target_pairs={{0,4},{4,0},{1,5},{5,1},{2,6},{6,2},{3,7},{7,3},{8,12},{12,8},{9,1... | collective-permute-start | bytes 1572872 | tf_op jit(solution)/shard_map/ppermute | solution.py:377
  42.3 15.5 %all-to-all-start.2 = ((f32[32,32,128]{2,1,0:T(8,128)}), f32[32,32,128]{2,1,0:T(8,128)S(1)}, u32[]{:S(2)}, u32[]{:S(2)}) async-start(f32[32,32,128]{2,1,0:T(8,128)} %get-tuple-element.44), calls=%async_computation.2 | async-start | bytes 1048576 | tf_op jit(solution)/shard_map/all_to_all | solution.py:349
  46.2 1.0 %copy-start.10 = (f32[128,512]{1,0:T(8,128)S(1)}, f32[128,512]{1,0:T(8,128)}, u32[]{:S(2)}) copy-start(f32[128,512]{1,0:T(8,128)} %copy-done.9) | copy-start | bytes 786436
  47.1 0.9 %copy-start.12 = (f32[128,512]{1,0:T(8,128)S(1)}, f32[128,512]{1,0:T(8,128)}, u32[]{:S(2)}) copy-start(f32[128,512]{1,0:T(8,128)} %copy-done.11) | copy-start | bytes 786436
  48.1 0.9 copy-start.18
  49.0 0.9 copy-start.20
  50.3 0.7 copy-start.15
  57.7 0.9 copy-start.14
  58.8 19.5 %copy-start = (bf16[1024,256]{1,0:T(8,128)(2,1)S(1)}, bf16[1024,256]{1,0:T(8,128)(2,1)}, u32[]{:S(2)}) copy-start(bf16[1024,256]{1,0:T(8,128)(2,1)} %wf_hbm.3) | copy-start | bytes 1572868
  58.8 19.5 %copy-start.1 = (bf16[1024,256]{1,0:T(8,128)(2,1)S(1)}, bf16[1024,256]{1,0:T(8,128)(2,1)}, u32[]{:S(2)}) copy-start(bf16[1024,256]{1,0:T(8,128)(2,1)} %wb_hbm.3) | copy-start | bytes 1572868
  58.8 19.5 %copy-start.2 = (bf16[1024,256]{1,0:T(8,128)(2,1)S(1)}, bf16[1024,256]{1,0:T(8,128)(2,1)}, u32[]{:S(2)}) copy-start(bf16[1024,256]{1,0:T(8,128)(2,1)} %wv_hbm.3) | copy-start | bytes 1572868
  58.8 19.5 %copy-start.16 = (f32[128,256]{1,0:T(8,128)S(1)}, f32[128,256]{1,0:T(8,128)}, u32[]{:S(2)}) copy-start(f32[128,256]{1,0:T(8,128)} %copy-done.15) | copy-start | bytes 393220
  58.8 19.5 %copy-start.22 = (bf16[128,256]{1,0:T(8,128)(2,1)S(1)}, bf16[128,256]{1,0:T(8,128)(2,1)}, u32[]{:S(2)}) copy-start(bf16[128,256]{1,0:T(8,128)(2,1)} %get-tuple-element.33.v_ref) | copy-start | bytes 196612
  58.8 19.5 %copy-start.24 = (bf16[128,256]{1,0:T(8,128)(2,1)S(1)}, bf16[128,256]{1,0:T(8,128)(2,1)}, u32[]{:S(2)}) copy-start(bf16[128,256]{1,0:T(8,128)(2,1)} %copy-done.23) | copy-start | bytes 196612
where the time goes:
time: 95.9 us; the launch traced here: 94.8 us
  blocking collectives  51.7 us (54%)
  waiting for transfers between devices  12.5 us (13%)
  Pallas kernels  12 us (13%)
  local copies, waits for them, and re-layouts  9.18 us (10%)
  starting transfers between devices  7.85 us (8%)
    all_to_all x3, blocking collectives, exchange(): return lax.all_to_all(array, axes, 0, 0, tiled=True)  51.7 us
    all_to_all x2, waiting for transfers between devices, exchange(): return lax.all_to_all(array, axes, 0, 0, tiled=True)  12.5 us
    unnamed x56, local copies, waits for them, and re-layouts  9.18 us
    all_to_all x2, starting transfers between devices, exchange(): return lax.all_to_all(array, axes, 0, 0, tiled=True)  7.71 us
    pallas_call x1, Pallas kernels, body(): call(project_kernel, (tok16, tok16, tok16, tok, tok, shape(N, 24, K)), [H...  3.6 us
    pallas_call x1, Pallas kernels, body(): call(finish_kernel, (shape(T, D), shape(N, W), shape(2, W)), [VMEM] * 12...  2.46 us
    pallas_call x1, Pallas kernels, body(): call(query_kernel, (shape(N, 32, K), shape(N, 32, K), tok16, wide, wide),...  1.92 us
  transfers between devices with their start and end apart: 3, of which 2 were waited for; matrix products, arithmetic and copies ran while one was open for 0% of the time, Pallas kernels for 2%

commit v1 on v0

--- a/solution.py
+++ b/solution.py
@@ -91,7 +91,7 @@
 
 
 def project_kernel(
-    x_hbm, wf_hbm, wb_hbm, wv_hbm, rate_hbm, f_ref, b_ref, v_ref, cf_ref, cb_ref, msg_ref, x_buf, w_buf, rate_buf, sems
+    x_hbm, wf_hbm, wb_hbm, wv_hbm, rate_hbm, f_ref, b_ref, v_ref, msg_ref, x_buf, w_buf, rate_buf, sems
 ):
     get_x, get_wf, get_rate, get_wb, get_wv = fetch(
         (x_hbm, wf_hbm, rate_hbm, wb_hbm, wv_hbm), (x_buf, w_buf.at[0], rate_buf, w_buf.at[1], w_buf.at[2]), sems
@@ -101,12 +101,11 @@
     low, up = low.astype(BF16), up.astype(BF16)
     opening = opening_of(get_rate())
     decayed = []
-    for d, (get_w, raw_ref, cum_ref, tri) in enumerate(((get_wf, f_ref, cf_ref, low), (get_wb, b_ref, cb_ref, up))):
+    for d, (get_w, raw_ref, tri) in enumerate(((get_wf, f_ref, low), (get_wb, b_ref, up))):
         raw = dot(x, get_w(), NN).astype(BF16)
         raw_ref[...] = raw
         _, key = gates(raw, opening[d : d + 1])
         cum = dot2(tri, log_forget_of(key), NN)
-        cum_ref[...] = cum
         last = cum[T - 1 : T] if d == 0 else cum[0:1]
         decayed.append((jnp.exp(last), key * jnp.exp(last - cum)))
     v = dot(x, get_wv(), NN).astype(BF16)
@@ -123,8 +122,8 @@
 
 
 def local_kernel(
-    x_hbm, wq_hbm, f_ref, b_ref, v_ref, cf_ref, cb_ref, rate_ref, gain_ref, cot_ref,
-    a_ref, scores_ref, inner_ref, reach_ref, tail_ref, share_ref, scaled_ref, x_buf, w_buf, sems,
+    x_hbm, wq_hbm, f_ref, b_ref, v_ref, rate_ref, gain_ref, cot_ref,
+    cf_ref, cb_ref, a_ref, bk_ref, scores_ref, inner_ref, reach_ref, tail_ref, share_ref, scaled_ref, x_buf, w_buf, sems,
 ):
     get_x, get_wq = fetch((x_hbm, wq_hbm), (x_buf, w_buf), sems)
     low, up = lower_triangle()
@@ -138,13 +137,15 @@
         zs = []
         for d, (raw_ref, cum_ref, tri) in enumerate(((f_ref, cf_ref, low), (b_ref, cb_ref, up))):
             closed, key = gates(raw_ref[:, cols], opening[d : d + 1, cols])
-            cum = cum_ref[:, cols]
+            cum = dot2(tri.astype(BF16), log_forget_of(key), NN)
+            cum_ref[:, cols] = cum
             fade = jnp.exp(-cum)
             last = cum[T - 1 : T] if d == 0 else cum[0:1]
             a = query[:, cols] * jnp.exp(cum)
             b = key * fade
             both = slice((2 * h + d) * K, (2 * h + d + 1) * K)
             a_ref[:, both] = a
+            bk_ref[:, both] = b
             scores = scores + jnp.where(tri, dot3(a, b, NT), 0.0)
             share = closed / (1.0 - key)
             before = dot2(tri.astype(BF16), share, NN)
@@ -159,8 +160,7 @@
         reach_ref[:, 2 * h * K : 2 * (h + 1) * K] = dot2(v_t, jnp.concatenate(zs, axis=1), NN)
 
 
-def scan_kernel(got_ref, out_ref, keep_ref):
-    keep_ref[...] = got_ref[:, 16:24, :]
+def scan_kernel(got_ref, out_ref):
     run_f = run_b = jnp.zeros((8, K), F32)
     for i in range(N):
         j = N - 1 - i
@@ -197,30 +197,25 @@
 
 
 def query_kernel(
-    core_ref, x_hbm, f_ref, b_ref, cf_ref, cb_ref, rate_ref, v_ref, a_ref, in_ref, dm_ref,
+    core_ref, x_hbm, cf_ref, cb_ref, v_ref, a_ref, bk_ref, in_ref, dm_ref,
     own_ref, other_ref, gq_ref, local_ref, ada_ref, x_buf, sems,
 ):
     (get_x,) = fetch((x_hbm,), (x_buf,), sems)
     low, up = lower_triangle()
-    opening = opening_of(rate_ref[...])
     grad_q = []
     for h in range(HEADS):
         cols = slice(h * K, (h + 1) * K)
         d_mixed = dm_ref[:, cols]
         d_scores = dot2r(d_mixed, v_ref[:, cols], NT)
         dq = jnp.zeros((T, K), F32)
-        for d, (state, raw_ref, cum_ref, tri) in enumerate(
-            zip(states_of(in_ref, h), (f_ref, b_ref), (cf_ref, cb_ref), (low, up))
-        ):
-            _, key = gates(raw_ref[:, cols], opening[d : d + 1, cols])
-            cum = cum_ref[:, cols]
+        for d, (state, cum_ref, tri) in enumerate(zip(states_of(in_ref, h), (cf_ref, cb_ref), (low, up))):
             both = slice((2 * h + d) * K, (2 * h + d + 1) * K)
             local = jnp.where(tri, d_scores, 0.0)
             local_ref[:, both] = local
             da = dot3(
-                jnp.concatenate([local, d_mixed], axis=1), jnp.concatenate([key * jnp.exp(-cum), state], axis=0), NN
+                jnp.concatenate([local, d_mixed], axis=1), jnp.concatenate([bk_ref[:, both], state], axis=0), NN
             )
-            dq = dq + da * jnp.exp(cum)
+            dq = dq + da * jnp.exp(cum_ref[:, cols])
             ada_ref[:, both] = a_ref[:, both] * da
         grad_q.append((dq * Q_SCALE).astype(BF16))
     gq = jnp.concatenate(grad_q, axis=1)
@@ -235,7 +230,7 @@
 
 
 def key_kernel(
-    f_ref, b_ref, cf_ref, cb_ref, rate_ref, a_ref, scores_ref, share_ref, local_ref, ada_ref, dm_ref,
+    f_ref, b_ref, cf_ref, cb_ref, rate_ref, a_ref, bk_ref, scores_ref, share_ref, local_ref, ada_ref, dm_ref,
     db_ref, dv_ref, floor_ref,
 ):
     opening = opening_of(rate_ref[...])
@@ -246,9 +241,10 @@
             both = slice((2 * h + d) * K, (2 * h + d + 1) * K)
             db = dot3(local_ref[:, both].T, a_ref[:, both], NN)
             db_ref[:, both] = db
-            closed, key = gates(raw_ref[:, cols], opening[d : d + 1, cols])
-            faded = db * jnp.exp(-cum_ref[:, cols])
-            floor = closed * faded - share_ref[:, both] * (ada_ref[:, both] - key * faded)
+            closed, _ = gates(raw_ref[:, cols], opening[d : d + 1, cols])
+            floor = closed * (db * jnp.exp(-cum_ref[:, cols])) - share_ref[:, both] * (
+                ada_ref[:, both] - bk_ref[:, both] * db
+            )
             floor_ref[2 * h + d : 2 * h + d + 1, :] = jnp.sum(floor, axis=0, keepdims=True)
 
 
@@ -260,8 +256,8 @@
         out_ref[i, 8:16, :] = run_b
         reach_f = reach_f + run_f * got_ref[j, 16:24, :]
         reach_b = reach_b + run_b * got_ref[i, 24:32, :]
-        run_f = keep_ref[j, 0:1, :] * run_f + got_ref[j, 0:8, :]
-        run_b = keep_ref[i, 1:2, :] * run_b + got_ref[i, 8:16, :]
+        run_f = keep_ref[j, 16:17, :] * run_f + got_ref[j, 0:8, :]
+        run_b = keep_ref[i, 17:18, :] * run_b + got_ref[i, 8:16, :]
     out_ref[:, 16:48, :] = own_ref[...] + other_ref[...]
     tail = [jnp.sum(reach_f, axis=0, keepdims=True), jnp.sum(reach_b, axis=0, keepdims=True)]
     tail = jnp.concatenate(tail + [local_ref[...], jnp.zeros((2, K), F32)], axis=0)
@@ -354,31 +350,30 @@
     tok16 = shape(T, W, dtype=BF16)
     x_buf, w_buf = pltpu.VMEM((T, D), BF16), pltpu.VMEM((D, W), BF16)
     dma = pltpu.SemaphoreType.DMA
-    f, b, v, cf, cb, sums = call(
-        project_kernel, (tok16, tok16, tok16, tok, tok, shape(N, 24, K)), [HBM] * 5, MANY,
+    f, b, v, sums = call(
+        project_kernel, (tok16, tok16, tok16, shape(N, 24, K)), [HBM] * 5, MANY,
         (x_buf, pltpu.VMEM((3, D, W), BF16), pltpu.VMEM((2, W), F32), dma((5,))), PROJECT_LIMIT,
     )(x, w_forget_fwd, w_forget_bwd, w_value, floor_rate)
     sums = exchange(sums, SP)
-    a, scores, inner, reach, tail, share, scaled = call(
-        local_kernel, (wide, tok, tok, wide, shape(4, K), wide, tok), [HBM] * 2 + [VMEM] * 8, MANY,
+    cf, cb, a, bk, scores, inner, reach, tail, share, scaled = call(
+        local_kernel, (tok, tok, wide, wide, tok, tok, wide, shape(4, K), wide, tok), [HBM] * 2 + [VMEM] * 6, MANY,
         (x_buf, w_buf, dma((2,))),
-    )(x, w_query, f, b, v, cf, cb, floor_rate, gain.reshape(1, K), cotangent)
-    inflow, keeps = call(scan_kernel, (shape(N, 16, K), shape(N, 8, K)), [VMEM], FEW)(sums)
-    inflow = exchange(inflow, SP)
+    )(x, w_query, f, b, v, floor_rate, gain.reshape(1, K), cotangent)
+    inflow = exchange(call(scan_kernel, shape(N, 16, K), [VMEM], FEW)(sums), SP)
     seeds, dm = call(mix_kernel, (shape(N, 32, K), tok), [VMEM] * 6, MANY)(
         a, inner, reach, tail, scaled, inflow
     )
     seeds = exchange(seeds, SP)
     core = lax.axis_index("sp_2").reshape(1).astype(jnp.int32)
     own, other, gq, local, ada = call(
-        query_kernel, (shape(N, 32, K), shape(N, 32, K), tok16, wide, wide), [SMEM, HBM] + [VMEM] * 9,
+        query_kernel, (shape(N, 32, K), shape(N, 32, K), tok16, wide, wide), [SMEM, HBM] + [VMEM] * 7,
         MANY, (x_buf, dma((1,))),
-    )(core, x, f, b, cf, cb, floor_rate, v, a, inflow, dm)
+    )(core, x, cf, cb, v, a, bk, inflow, dm)
     other = lax.ppermute(other, "sp_2", [(0, 1), (1, 0)])
-    db, dv, floor = call(key_kernel, (wide, tok, shape(4, K)), [VMEM] * 11, MANY)(
-        f, b, cf, cb, floor_rate, a, scores, share, local, ada, dm
-    )
-    outflow = exchange(call(scan_back_kernel, shape(N, 56, K), [VMEM] * 5, FEW)(keeps, seeds, own, other, floor), SP)
+    db, dv, floor = call(key_kernel, (wide, tok, shape(4, K)), [VMEM] * 12, MANY)(
+        f, b, cf, cb, floor_rate, a, bk, scores, share, local, ada, dm
+    )
+    outflow = exchange(call(scan_back_kernel, shape(N, 56, K), [VMEM] * 5, FEW)(sums, seeds, own, other, floor), SP)
     term, grad_weight, grad_floor = call(
         finish_kernel, (shape(T, D), shape(N, W), shape(2, W)), [VMEM] * 12 + [HBM] * 4, MANY,
         (pltpu.VMEM((4, D, W), BF16), dma((4,))),

time: 95.9 us -> 94.6 us (0.986)
  waiting for transfers between devices: 12.5 us -> 10.9 us
    all_to_all x2, waiting for transfers between devices: 12.5 us -> 10.9 us  [exchange(): return lax.all_to_all(array, axes, 0, 0, tiled=True)]
    unnamed x56 -> x64, local copies, waits for them, and re-layouts: 9.18 us -> 9.93 us
where the time goes in v1:
time: 94.6 us; the launch traced here: 93.5 us
  blocking collectives  51.6 us (55%)
  Pallas kernels  11.4 us (12%)
  waiting for transfers between devices  10.9 us (12%)
  local copies, waits for them, and re-layouts  9.93 us (10%)
  starting transfers between devices  8.12 us (9%)
  between operations  0.96 us (1%)
    all_to_all x3, blocking collectives, exchange(): return lax.all_to_all(array, axes, 0, 0, tiled=True)  51.6 us
    all_to_all x2, waiting for transfers between devices, exchange(): return lax.all_to_all(array, axes, 0, 0, tiled=True)  10.9 us
    unnamed x64, local copies, waits for them, and re-layouts  9.93 us
    all_to_all x2, starting transfers between devices, exchange(): return lax.all_to_all(array, axes, 0, 0, tiled=True)  7.98 us
    pallas_call x1, Pallas kernels, body(): call(project_kernel, (tok16, tok16, tok16, shape(N, 24, K)), [HBM] * 5, M...  3.59 us
    pallas_call x1, Pallas kernels, body(): call(finish_kernel, (shape(T, D), shape(N, W), shape(2, W)), [VMEM] * 12...  2.45 us
    pallas_call x1, Pallas kernels, body(): call(query_kernel, (shape(N, 32, K), shape(N, 32, K), tok16, wide, wide),...  1.94 us
  transfers between devices with their start and end apart: 3, of which 2 were waited for; matrix products, arithmetic and copies ran while one was open for 0% of the time, Pallas kernels for 2%

profile of v1, /device:TPU:1, one launch (start us, length us, event | category | flops | bytes accessed | tf_op | source)
XLA Modules:
  0.0 93.5 jit_solution(9105946251431430154)
XLA Ops:
  0.6 3.6 %shard_map.103 = (bf16[128,256]{1,0:T(8,128)(2,1)}, bf16[128,256]{1,0:T(8,128)(2,1)}, bf16[128,256]{1,0:T(8,128)(2,1)}, f32[32,24,128]{2,1,0:T(8,128)}) custom-call(bf16[128,1024]{1,0:T(8,128)(2,1)} %x_hbm.5, bf16[1024,256]{1,0:T(8,128)(2,1)} %wf_hbm.3, bf16[1024,256]{1,0:T(8,128)(2,1)} %wb_hbm.3, bf16[1024,256]{1,0:T(8,128)(2,1)} %wv_hbm.3, f32[2,256]{1,0:T(2,128)} %rate_ref.5), custom_call_target="tpu_custom_call" | custom-call | flops 400000000 | bytes 1048576 | tf_op jit(solution)/shard_map/pallas_call | solution.py:353
  4.2 18.7 %all_to_all.29.got_ref.keep_ref = f32[32,24,128]{2,1,0:T(8,128)S(1)} all-to-all(f32[32,24,128]{2,1,0:T(8,128)} %get-tuple-element.35), channel_id=1, replica_groups=mesh['sp_0'=4,'sp_1'=4,'sp_2'=2,'tp'=4] {'sp_0','sp_1','sp_2'}, dimensions={0} | all-to-all | bytes 786432 | tf_op jit(solution)/shard_map/all_to_all | solution.py:345
  23.0 0.8 shard_map.105
  23.7 0.0 copy-start.30
  23.7 3.9 %all-to-all-start.1 = ((f32[32,16,128]{2,1,0:T(8,128)}), f32[32,16,128]{2,1,0:T(8,128)S(1)}, u32[]{:S(2)}, u32[]{:S(2)}) async-start(f32[32,16,128]{2,1,0:T(8,128)} %shard_map.105), calls=%async_computation.1 | async-start | bytes 524288 | tf_op jit(solution)/shard_map/all_to_all | solution.py:345
  27.7 0.0 copy-start.29
  27.7 0.0 copy-start.31
  27.7 0.0 copy-done.7
  27.7 0.0 copy-done.3
  27.7 0.0 copy-done.9
  27.7 0.0 copy-done.12
  27.8 0.0 copy-done.15
  27.8 0.0 copy-done.30
  27.8 0.6 copy-done.29
  28.4 0.0 copy-done.31
  28.4 1.4 %shard_map.104 = (f32[128,256]{1,0:T(8,128)S(1)}, f32[128,256]{1,0:T(8,128)S(1)}, f32[128,512]{1,0:T(8,128)S(1)}, f32[128,512]{1,0:T(8,128)S(1)}, f32[128,256]{1...) custom-call(bf16[128,1024]{1,0:T(8,128)(2,1)S(1)} %copy-done.3, ...), custom_call_target="tpu_custom_call" | custom-call | flops 400000000 | bytes 1048576 | tf_op jit(solution)/shard_map/pallas_call | solution.py:358
  29.8 0.0 copy-start.17
  29.8 0.7 copy-done.17
  30.5 0.6 copy-done.23
  31.1 5.5 %all-to-all-done.1.in_ref = f32[32,16,128]{2,1,0:T(8,128)S(1)} async-done(((f32[32,16,128]{2,1,0:T(8,128)}), f32[32,16,128]{2,1,0:T(8,128)S(1)}, u32[]{:S(2)}, u32[]{:S(2)}) %all-to-all-start.1) | async-done | bytes 262176 | tf_op jit(solution)/shard_map/all_to_all | solution.py:345
  36.7 0.7 shard_map.106
  37.4 0.0 copy-start.4
  37.4 0.8 copy-done.4
  38.2 1.9 %shard_map.107 = (f32[32,32,128]{2,1,0:T(8,128)S(1)}, f32[32,32,128]{2,1,0:T(8,128)}, bf16[128,256]{1,0:T(8,128)(2,1)S(1)}, f32[128,512]{1,0:T(8,128)S(1)}, f32[128,512]{1,0:T(8,128)S(1)}) custom-call(s32[1]{0:T(128)} %bitcast.1.core_ref, bf16[128,1024]{1,0:T(8,128)(2,1)S(1)} %copy-done.3, f32[128,256]{1,0:T(8,128)S(1)} %get-tuple-element.33.cf_ref, ...), custom_call_target="tpu_custom_call" | custom-call | flops 400000000 | bytes 1048576 | tf_op jit(solution)/shard_map/pallas_call | solution.py:368
  40.2 0.7 copy-done.21
  40.9 0.6 copy-done.27
  41.5 0.1 collective-permute-start
  41.6 4.0 %all-to-all-start.2 = ((f32[32,32,128]{2,1,0:T(8,128)}), f32[32,32,128]{2,1,0:T(8,128)S(1)}, u32[]{:S(2)}, u32[]{:S(2)}) async-start(f32[32,32,128]{2,1,0:T(8,128)} %copy-done.4), calls=%async_computation.2 | async-start | bytes 1048576 | tf_op jit(solution)/shard_map/all_to_all | solution.py:345
  45.7 0.9 copy-done.6
  46.6 0.8 copy-done.10
  47.5 0.8 copy-done.13
  48.3 0.9 %copy-done.22 = f32[128,512]{1,0:T(8,128)S(1)} copy-done((f32[128,512]{1,0:T(8,128)S(1)}, f32[128,512]{1,0:T(8,128)}, u32[]{:S(2)}) %copy-start.22) | copy-done | bytes 262168
  49.2 0.9 copy-done.24
  50.1 0.4 shard_map.108
  50.6 0.7 copy-done.19
  51.3 0.6 copy-done.25
  51.9 5.3 %all-to-all-done.2.got_ref = f32[32,32,128]{2,1,0:T(8,128)S(1)} async-done(((f32[32,32,128]{2,1,0:T(8,128)}), f32[32,32,128]{2,1,0:T(8,128)S(1)}, u32[]{:S(2)}, u32[]{:S(2)}) %all-to-all-start.2) | async-done | bytes 524320 | tf_op jit(solution)/shard_map/all_to_all | solution.py:345
  57.2 0.0 collective-permute-done.other_ref
  57.3 0.1 shard_map.109
  57.4 0.0 copy-start
  57.4 0.0 copy-start.1
  57.4 0.0 copy-start.2
  57.4 0.0 copy-start.11
  57.4 19.4 %all_to_all.30.got_ref = f32[32,56,128]{2,1,0:T(8,128)S(1)} all-to-all(f32[32,56,128]{2,1,0:T(8,128)S(1)} %shard_map.109), channel_id=1, replica_groups=mesh['sp_0'=4,'sp_1'=4,'sp_2'=2,'tp'=4] {'sp_0','sp_1','sp_2'}, dimensions={0} | all-to-all | bytes 1835008 | tf_op jit(solution)/shard_map/all_to_all | solution.py:345
  76.8 0.0 copy-done.8
  76.9 2.5 %shard_map.110 = (f32[128,1024]{1,0:T(8,128)S(1)}, f32[32,256]{1,0:T(8,128)}, f32[2,256]{1,0:T(2,128)}) custom-call(bf16[128,256]{1,0:T(8,128)(2,1)S(1)} %copy-done.11, bf16[128,256]{1,0:T(8,128)(2,1)S(1)} %copy-done.14, bf16[128,256]{1,0:T(8,128)(2,1)S(1)} %copy-done.16, f32[128,256]{1,0:T(8,128)S(1)} %get-tuple-element.33.cf_ref, ...), custom_call_target="tpu_custom_call" | custom-call | flops 400000000 | bytes 1048576 | tf_op jit(solution)/shard_map/pallas_call | solution.py:377
  79.4 13.4 %all_to_all.31 = f32[4,32,1024]{2,1,0:T(8,128)S(1)} all-to-all(f32[4,32,1024]{2,1,0:T(8,128)S(1)} %bitcast.5), channel_id=1, replica_groups=mesh['sp_0'=4,'sp_1'=4,'sp_2'=2,'tp'=4] {'tp'}, dimensions={0} | all-to-all | bytes 1048576 | tf_op jit(solution)/shard_map/all_to_all | solution.py:345
  92.8 0.7 fusion.1
  (34 shorter events, 0.1 us)
Async XLA Ops:
  23.0 4.8 %copy-start.7 = (bf16[1024,256]{1,0:T(8,128)(2,1)S(1)}, bf16[1024,256]{1,0:T(8,128)(2,1)}, u32[]{:S(2)}) copy-start(bf16[1024,256]{1,0:T(8,128)(2,1)} %wq_hbm.3) | copy-start | bytes 1572868
  23.7 4.0 %copy-start.3 = (bf16[128,1024]{1,0:T(8,128)(2,1)S(1)}, bf16[128,1024]{1,0:T(8,128)(2,1)}, u32[]{:S(2)}) copy-start(bf16[128,1024]{1,0:T(8,128)(2,1)} %x_hbm.5) | copy-start | bytes 786436
  23.7 4.0 %copy-start.9 = (bf16[128,256]{1,0:T(8,128)(2,1)S(1)}, bf16[128,256]{1,0:T(8,128)(2,1)}, u32[]{:S(2)}) copy-start(bf16[128,256]{1,0:T(8,128)(2,1)} %get-tuple-element.30.f_ref) | copy-start | bytes 196612
  23.7 4.0 %copy-start.12 = (bf16[128,256]{1,0:T(8,128)(2,1)S(1)}, bf16[128,256]{1,0:T(8,128)(2,1)}, u32[]{:S(2)}) copy-start(bf16[128,256]{1,0:T(8,128)(2,1)} %get-tuple-element.31.b_ref) | copy-start | bytes 196612
  23.7 4.0 %copy-start.15 = (bf16[128,256]{1,0:T(8,128)(2,1)S(1)}, bf16[128,256]{1,0:T(8,128)(2,1)}, u32[]{:S(2)}) copy-start(bf16[128,256]{1,0:T(8,128)(2,1)} %get-tuple-element.32.v_ref) | copy-start | bytes 196612
  23.7 4.0 %copy-start.30 = (bf16[128,256]{1,0:T(8,128)(2,1)S(1)}, bf16[128,256]{1,0:T(8,128)(2,1)}, u32[]{:S(2)}) copy-start(bf16[128,256]{1,0:T(8,128)(2,1)} %cot_ref.1) | copy-start | bytes 196612
  23.7 12.9 %all-to-all-start.1 = ((f32[32,16,128]{2,1,0:T(8,128)}), f32[32,16,128]{2,1,0:T(8,128)S(1)}, u32[]{:S(2)}, u32[]{:S(2)}) async-start(f32[32,16,128]{2,1,0:T(8,128)} %shard_map.105), calls=%async_computation.1 | async-start | bytes 524288 | tf_op jit(solution)/shard_map/all_to_all | solution.py:345
  27.7 0.7 copy-start.29
  27.7 0.7 copy-start.31
  29.8 0.7 copy-start.17
  30.5 0.7 copy-start.23
  37.4 0.8 copy-start.4
  38.2 1.9 %copy-start.5 = (f32[128,256]{1,0:T(8,128)}, f32[128,256]{1,0:T(8,128)S(1)}, u32[]{:S(2)}) copy-start(f32[128,256]{1,0:T(8,128)S(1)} %get-tuple-element.43.dm_ref) | copy-start | bytes 393220
  40.2 0.7 copy-start.21
  40.9 0.6 copy-start.27
  41.5 15.7 %collective-permute-start = (f32[32,32,128]{2,1,0:T(8,128)}, f32[32,32,128]{2,1,0:T(8,128)S(1)}, u32[]{:S(2)}, u32[]{:S(2)}) collective-permute-start(f32[32,32,128]{2,1,0:T(8,128)} %get-tuple-element.45), channel_id=1, source_target_pairs={{0,4},{4,0},{1,5},{5,1},{2,6},{6,2},{3,7},{7,3},{8,12},{12,8},{9,1... | collective-permute-start | bytes 1572872 | tf_op jit(solution)/shard_map/ppermute | solution.py:372
  41.6 4.1 %copy-start.18 = (f32[128,512]{1,0:T(8,128)S(1)}, f32[128,512]{1,0:T(8,128)}, u32[]{:S(2)}) copy-start(f32[128,512]{1,0:T(8,128)} %copy-done.17) | copy-start | bytes 786436
  41.6 15.6 %all-to-all-start.2 = ((f32[32,32,128]{2,1,0:T(8,128)}), f32[32,32,128]{2,1,0:T(8,128)S(1)}, u32[]{:S(2)}, u32[]{:S(2)}) async-start(f32[32,32,128]{2,1,0:T(8,128)} %copy-done.4), calls=%async_computation.2 | async-start | bytes 1048576 | tf_op jit(solution)/shard_map/all_to_all | solution.py:345
  45.7 0.9 copy-start.6
  46.6 0.8 copy-start.10
  47.5 0.8 copy-start.13
  48.3 0.9 %copy-start.22 = (f32[128,512]{1,0:T(8,128)S(1)}, f32[128,512]{1,0:T(8,128)}, u32[]{:S(2)}) copy-start(f32[128,512]{1,0:T(8,128)} %copy-done.21) | copy-start | bytes 786436
  49.2 0.9 copy-start.24
  50.6 0.7 copy-start.19
  51.3 0.6 copy-start.25
  57.2 19.6 %copy-start.8 = (bf16[1024,256]{1,0:T(8,128)(2,1)S(1)}, bf16[1024,256]{1,0:T(8,128)(2,1)}, u32[]{:S(2)}) copy-start(bf16[1024,256]{1,0:T(8,128)(2,1)} %wq_hbm.3) | copy-start | bytes 1572868
  57.2 19.6 %copy-start.20 = (f32[128,512]{1,0:T(8,128)S(1)}, f32[128,512]{1,0:T(8,128)}, u32[]{:S(2)}) copy-start(f32[128,512]{1,0:T(8,128)} %copy-done.19) | copy-start | bytes 786436
  57.2 19.6 %copy-start.26 = (f32[128,256]{1,0:T(8,128)S(1)}, f32[128,256]{1,0:T(8,128)}, u32[]{:S(2)}) copy-start(f32[128,256]{1,0:T(8,128)} %copy-done.25) | copy-start | bytes 393220
  57.4 19.5 %copy-start = (bf16[1024,256]{1,0:T(8,128)(2,1)S(1)}, bf16[1024,256]{1,0:T(8,128)(2,1)}, u32[]{:S(2)}) copy-start(bf16[1024,256]{1,0:T(8,128)(2,1)} %wf_hbm.3) | copy-start | bytes 1572868
  57.4 19.5 %copy-start.1 = (bf16[1024,256]{1,0:T(8,128)(2,1)S(1)}, bf16[1024,256]{1,0:T(8,128)(2,1)}, u32[]{:S(2)}) copy-start(bf16[1024,256]{1,0:T(8,128)(2,1)} %wb_hbm.3) | copy-start | bytes 1572868
  57.4 19.5 %copy-start.2 = (bf16[1024,256]{1,0:T(8,128)(2,1)S(1)}, bf16[1024,256]{1,0:T(8,128)(2,1)}, u32[]{:S(2)}) copy-start(bf16[1024,256]{1,0:T(8,128)(2,1)} %wv_hbm.3) | copy-start | bytes 1572868
  57.4 19.5 %copy-start.11 = (bf16[128,256]{1,0:T(8,128)(2,1)S(1)}, bf16[128,256]{1,0:T(8,128)(2,1)}, u32[]{:S(2)}) copy-start(bf16[128,256]{1,0:T(8,128)(2,1)} %get-tuple-element.30.f_ref) | copy-start | bytes 196612
  57.4 19.5 %copy-start.14 = (bf16[128,256]{1,0:T(8,128)(2,1)S(1)}, bf16[128,256]{1,0:T(8,128)(2,1)}, u32[]{:S(2)}) copy-start(bf16[128,256]{1,0:T(8,128)(2,1)} %get-tuple-element.31.b_ref) | copy-start | bytes 196612
  57.4 19.5 %copy-start.16 = (bf16[128,256]{1,0:T(8,128)(2,1)S(1)}, bf16[128,256]{1,0:T(8,128)(2,1)}, u32[]{:S(2)}) copy-start(bf16[128,256]{1,0:T(8,128)(2,1)} %get-tuple-element.32.v_ref) | copy-start | bytes 196612
  57.4 19.5 %copy-start.28 = (bf16[128,256]{1,0:T(8,128)(2,1)S(1)}, bf16[128,256]{1,0:T(8,128)(2,1)}, u32[]{:S(2)}) copy-start(bf16[128,256]{1,0:T(8,128)(2,1)} %copy-done.27) | copy-start | bytes 196612

commit v2 on v1

--- a/solution.py
+++ b/solution.py
@@ -26,7 +26,7 @@
 VMEM = pl.BlockSpec(memory_space=pltpu.VMEM)
 SMEM = pl.BlockSpec(memory_space=pltpu.SMEM)
 HBM = pl.BlockSpec(memory_space=pltpu.HBM)
-VMEM_LIMIT = 8 << 20
+VMEM_LIMIT = 5 << 20
 PROJECT_LIMIT = 67043328 - (900 << 10)
 MANY, FEW = 400_000_000, 10_000_000
 
@@ -91,7 +91,7 @@
 
 
 def project_kernel(
-    x_hbm, wf_hbm, wb_hbm, wv_hbm, rate_hbm, f_ref, b_ref, v_ref, msg_ref, x_buf, w_buf, rate_buf, sems
+    x_hbm, wf_hbm, wb_hbm, wv_hbm, rate_hbm, f_ref, b_ref, v_ref, cf_ref, cb_ref, msg_ref, x_buf, w_buf, rate_buf, sems
 ):
     get_x, get_wf, get_rate, get_wb, get_wv = fetch(
         (x_hbm, wf_hbm, rate_hbm, wb_hbm, wv_hbm), (x_buf, w_buf.at[0], rate_buf, w_buf.at[1], w_buf.at[2]), sems
@@ -101,11 +101,12 @@
     low, up = low.astype(BF16), up.astype(BF16)
     opening = opening_of(get_rate())
     decayed = []
-    for d, (get_w, raw_ref, tri) in enumerate(((get_wf, f_ref, low), (get_wb, b_ref, up))):
+    for d, (get_w, raw_ref, cum_ref, tri) in enumerate(((get_wf, f_ref, cf_ref, low), (get_wb, b_ref, cb_ref, up))):
         raw = dot(x, get_w(), NN).astype(BF16)
         raw_ref[...] = raw
         _, key = gates(raw, opening[d : d + 1])
         cum = dot2(tri, log_forget_of(key), NN)
+        cum_ref[...] = cum
         last = cum[T - 1 : T] if d == 0 else cum[0:1]
         decayed.append((jnp.exp(last), key * jnp.exp(last - cum)))
     v = dot(x, get_wv(), NN).astype(BF16)
@@ -122,8 +123,8 @@
 
 
 def local_kernel(
-    x_hbm, wq_hbm, f_ref, b_ref, v_ref, rate_ref, gain_ref, cot_ref,
-    cf_ref, cb_ref, a_ref, bk_ref, scores_ref, inner_ref, reach_ref, tail_ref, share_ref, scaled_ref, x_buf, w_buf, sems,
+    x_hbm, wq_hbm, f_ref, b_ref, v_ref, cf_ref, cb_ref, rate_ref, gain_ref, cot_ref,
+    a_ref, bk_ref, scores_ref, inner_ref, reach_ref, tail_ref, share_ref, scaled_ref, x_buf, w_buf, sems,
 ):
     get_x, get_wq = fetch((x_hbm, wq_hbm), (x_buf, w_buf), sems)
     low, up = lower_triangle()
@@ -137,8 +138,7 @@
         zs = []
         for d, (raw_ref, cum_ref, tri) in enumerate(((f_ref, cf_ref, low), (b_ref, cb_ref, up))):
             closed, key = gates(raw_ref[:, cols], opening[d : d + 1, cols])
-            cum = dot2(tri.astype(BF16), log_forget_of(key), NN)
-            cum_ref[:, cols] = cum
+            cum = cum_ref[:, cols]
             fade = jnp.exp(-cum)
             last = cum[T - 1 : T] if d == 0 else cum[0:1]
             a = query[:, cols] * jnp.exp(cum)
@@ -350,15 +350,15 @@
     tok16 = shape(T, W, dtype=BF16)
     x_buf, w_buf = pltpu.VMEM((T, D), BF16), pltpu.VMEM((D, W), BF16)
     dma = pltpu.SemaphoreType.DMA
-    f, b, v, sums = call(
-        project_kernel, (tok16, tok16, tok16, shape(N, 24, K)), [HBM] * 5, MANY,
+    f, b, v, cf, cb, sums = call(
+        project_kernel, (tok16, tok16, tok16, tok, tok, shape(N, 24, K)), [HBM] * 5, MANY,
         (x_buf, pltpu.VMEM((3, D, W), BF16), pltpu.VMEM((2, W), F32), dma((5,))), PROJECT_LIMIT,
     )(x, w_forget_fwd, w_forget_bwd, w_value, floor_rate)
     sums = exchange(sums, SP)
-    cf, cb, a, bk, scores, inner, reach, tail, share, scaled = call(
-        local_kernel, (tok, tok, wide, wide, tok, tok, wide, shape(4, K), wide, tok), [HBM] * 2 + [VMEM] * 6, MANY,
+    a, bk, scores, inner, reach, tail, share, scaled = call(
+        local_kernel, (wide, wide, tok, tok, wide, shape(4, K), wide, tok), [HBM] * 2 + [VMEM] * 8, MANY,
         (x_buf, w_buf, dma((2,))),
-    )(x, w_query, f, b, v, floor_rate, gain.reshape(1, K), cotangent)
+    )(x, w_query, f, b, v, cf, cb, floor_rate, gain.reshape(1, K), cotangent)
     inflow = exchange(call(scan_kernel, shape(N, 16, K), [VMEM], FEW)(sums), SP)
     seeds, dm = call(mix_kernel, (shape(N, 32, K), tok), [VMEM] * 6, MANY)(
         a, inner, reach, tail, scaled, inflow

time: 94.6 us -> 94.7 us (level)
    unnamed x64 -> x68, local copies, waits for them, and re-layouts: 9.93 us -> 9.96 us
where the time goes in v2:
time: 94.7 us; the launch traced here: 93.6 us
  blocking collectives  51.7 us (55%)
  Pallas kernels  11.2 us (12%)
  waiting for transfers between devices  11 us (12%)
  local copies, waits for them, and re-layouts  9.96 us (11%)
  starting transfers between devices  8.11 us (9%)
  between operations  0.98 us (1%)
    all_to_all x3, blocking collectives, exchange(): return lax.all_to_all(array, axes, 0, 0, tiled=True)  51.7 us
    all_to_all x2, waiting for transfers between devices, exchange(): return lax.all_to_all(array, axes, 0, 0, tiled=True)  11 us
    unnamed x68, local copies, waits for them, and re-layouts  9.96 us
    all_to_all x2, starting transfers between devices, exchange(): return lax.all_to_all(array, axes, 0, 0, tiled=True)  7.96 us
    pallas_call x1, Pallas kernels, body(): call(project_kernel, (tok16, tok16, tok16, tok, tok, shape(N, 24, K)), [H...  3.59 us
    pallas_call x1, Pallas kernels, body(): call(finish_kernel, (shape(T, D), shape(N, W), shape(2, W)), [VMEM] * 12...  2.44 us
    pallas_call x1, Pallas kernels, body(): call(query_kernel, (shape(N, 32, K), shape(N, 32, K), tok16, wide, wide),...  1.91 us
  transfers between devices with their start and end apart: 3, of which 2 were waited for; matrix products, arithmetic and copies ran while one was open for 0% of the time, Pallas kernels for 2%

profile of v2, /device:TPU:1, one launch (start us, length us, event | category | flops | bytes accessed | tf_op | source)
XLA Modules:
  0.0 93.6 jit_solution(7192117310615652407)
XLA Ops:
  0.6 3.6 %shard_map.103 = (bf16[128,256]{1,0:T(8,128)(2,1)}, bf16[128,256]{1,0:T(8,128)(2,1)}, bf16[128,256]{1,0:T(8,128)(2,1)}, f32[128,256]{1,0:T(8,128)}, f32[128,256]{1,0:T(8,128)}, /*index=5*/f32[32,24,128]{2,1,0:T(8,128)}) custom-call(bf16[128,1024]{1,0:T(8,128)(2,1)} %x_hbm.5, bf16[1024,256]{1,0:T(8,128)(2,1)} %wf_hbm.3, bf16[1024,256]{1,0:T(8,128)(2,1)} %wb_hbm.3, ...), custom_call_target="tpu_custom_call" | custom-call | flops 400000000 | bytes 1048576 | tf_op jit(solution)/shard_map/pallas_call | solution.py:353
  4.2 0.0 copy-start.32
  4.2 18.9 %all_to_all.29.got_ref.keep_ref = f32[32,24,128]{2,1,0:T(8,128)S(1)} all-to-all(f32[32,24,128]{2,1,0:T(8,128)} %get-tuple-element.35), channel_id=1, replica_groups=mesh['sp_0'=4,'sp_1'=4,'sp_2'=2,'tp'=4] {'sp_0','sp_1','sp_2'}, dimensions={0} | all-to-all | bytes 786432 | tf_op jit(solution)/shard_map/all_to_all | solution.py:345
  23.1 0.8 shard_map.104
  23.9 3.9 %all-to-all-start.1 = ((f32[32,16,128]{2,1,0:T(8,128)}), f32[32,16,128]{2,1,0:T(8,128)S(1)}, u32[]{:S(2)}, u32[]{:S(2)}) async-start(f32[32,16,128]{2,1,0:T(8,128)} %shard_map.104), calls=%async_computation.1 | async-start | bytes 524288 | tf_op jit(solution)/shard_map/all_to_all | solution.py:345
  27.8 0.0 copy-start.31
  27.8 0.0 copy-start.33
  27.8 0.0 copy-done.17
  27.9 0.0 copy-done.32
  27.9 0.0 copy-done.9
  27.9 0.0 copy-done.11
  27.9 0.0 copy-done.14
  27.9 0.0 copy-done.3
  27.9 0.0 copy-done.4
  27.9 0.0 copy-done.5
  27.9 0.6 copy-done.31
  28.5 1.2 %shard_map.105 = (f32[128,512]{1,0:T(8,128)S(1)}, f32[128,512]{1,0:T(8,128)S(1)}, f32[128,256]{1,0:T(8,128)S(1)}, f32[128,256]{1,0:T(8,128)S(1)}, f32[128,512]{1...) custom-call(bf16[128,1024]{1,0:T(8,128)(2,1)S(1)} %copy-done.5, ...), custom_call_target="tpu_custom_call" | custom-call | flops 400000000 | bytes 1048576 | tf_op jit(solution)/shard_map/pallas_call | solution.py:358
  29.7 0.7 copy-done.21
  30.4 0.6 copy-done.27
  31.1 5.7 %all-to-all-done.1.in_ref = f32[32,16,128]{2,1,0:T(8,128)S(1)} async-done(((f32[32,16,128]{2,1,0:T(8,128)}), f32[32,16,128]{2,1,0:T(8,128)S(1)}, u32[]{:S(2)}, u32[]{:S(2)}) %all-to-all-start.1) | async-done | bytes 262176 | tf_op jit(solution)/shard_map/all_to_all | solution.py:345
  36.8 0.7 shard_map.106
  37.5 0.0 copy-start.6
  37.5 0.8 copy-done.6
  38.3 1.9 %shard_map.107 = (f32[32,32,128]{2,1,0:T(8,128)S(1)}, f32[32,32,128]{2,1,0:T(8,128)}, bf16[128,256]{1,0:T(8,128)(2,1)S(1)}, f32[128,512]{1,0:T(8,128)S(1)}, f32[128,512]{1,0:T(8,128)S(1)}) custom-call(s32[1]{0:T(128)} %bitcast.1.core_ref, bf16[128,1024]{1,0:T(8,128)(2,1)S(1)} %copy-done.5, f32[128,256]{1,0:T(8,128)S(1)} %copy-done.3, ...), custom_call_target="tpu_custom_call" | custom-call | flops 400000000 | bytes 1048576 | tf_op jit(solution)/shard_map/pallas_call | solution.py:368
  40.3 0.7 copy-done.23
  41.0 0.6 copy-done.29
  41.6 0.1 collective-permute-start
  41.8 4.0 %all-to-all-start.2 = ((f32[32,32,128]{2,1,0:T(8,128)}), f32[32,32,128]{2,1,0:T(8,128)S(1)}, u32[]{:S(2)}, u32[]{:S(2)}) async-start(f32[32,32,128]{2,1,0:T(8,128)} %copy-done.6), calls=%async_computation.2 | async-start | bytes 1048576 | tf_op jit(solution)/shard_map/all_to_all | solution.py:345
  45.8 0.0 copy-done.22
  45.8 0.9 copy-done.8
  46.7 0.8 copy-done.12
  47.6 0.8 copy-done.15
  48.4 0.9 %copy-done.24 = f32[128,512]{1,0:T(8,128)S(1)} copy-done((f32[128,512]{1,0:T(8,128)S(1)}, f32[128,512]{1,0:T(8,128)}, u32[]{:S(2)}) %copy-start.24) | copy-done | bytes 262168
  49.4 0.9 copy-done.28
  50.3 0.4 shard_map.108
  50.7 0.7 copy-done.19
  51.4 0.7 copy-done.25
  52.1 5.3 %all-to-all-done.2.got_ref = f32[32,32,128]{2,1,0:T(8,128)S(1)} async-done(((f32[32,32,128]{2,1,0:T(8,128)}), f32[32,32,128]{2,1,0:T(8,128)S(1)}, u32[]{:S(2)}, u32[]{:S(2)}) %all-to-all-start.2) | async-done | bytes 524320 | tf_op jit(solution)/shard_map/all_to_all | solution.py:345
  57.4 0.0 collective-permute-done.other_ref
  57.4 0.1 shard_map.109
  57.5 0.0 copy-start
  57.5 0.0 copy-start.1
  57.5 0.0 copy-start.2
  57.5 0.0 copy-start.13
  57.6 19.4 %all_to_all.30.got_ref = f32[32,56,128]{2,1,0:T(8,128)S(1)} all-to-all(f32[32,56,128]{2,1,0:T(8,128)S(1)} %shard_map.109), channel_id=1, replica_groups=mesh['sp_0'=4,'sp_1'=4,'sp_2'=2,'tp'=4] {'sp_0','sp_1','sp_2'}, dimensions={0} | all-to-all | bytes 1835008 | tf_op jit(solution)/shard_map/all_to_all | solution.py:345
  77.1 2.4 %shard_map.110 = (f32[128,1024]{1,0:T(8,128)S(1)}, f32[32,256]{1,0:T(8,128)}, f32[2,256]{1,0:T(2,128)}) custom-call(bf16[128,256]{1,0:T(8,128)(2,1)S(1)} %copy-done.13, bf16[128,256]{1,0:T(8,128)(2,1)S(1)} %copy-done.16, bf16[128,256]{1,0:T(8,128)(2,1)S(1)} %copy-done.18, f32[128,256]{1,0:T(8,128)S(1)} %copy-done.3, f32[128,256]{1,0:T(8,128)S(1)} %copy-done.4, ...), custom_call_target="tpu_custom_call" | custom-call | flops 400000000 | bytes 1048576 | tf_op jit(solution)/shard_map/pallas_call | solution.py:377
  79.5 13.4 %all_to_all.31 = f32[4,32,1024]{2,1,0:T(8,128)S(1)} all-to-all(f32[4,32,1024]{2,1,0:T(8,128)S(1)} %bitcast.5), channel_id=1, replica_groups=mesh['sp_0'=4,'sp_1'=4,'sp_2'=2,'tp'=4] {'tp'}, dimensions={0} | all-to-all | bytes 1048576 | tf_op jit(solution)/shard_map/all_to_all | solution.py:345
  92.9 0.7 fusion.1
  (38 shorter events, 0.1 us)
Async XLA Ops:
  4.2 23.6 %copy-start.17 = (bf16[128,256]{1,0:T(8,128)(2,1)S(1)}, bf16[128,256]{1,0:T(8,128)(2,1)}, u32[]{:S(2)}) copy-start(bf16[128,256]{1,0:T(8,128)(2,1)} %get-tuple-element.32.v_ref) | copy-start | bytes 196612
  4.2 23.6 %copy-start.32 = (bf16[128,256]{1,0:T(8,128)(2,1)S(1)}, bf16[128,256]{1,0:T(8,128)(2,1)}, u32[]{:S(2)}) copy-start(bf16[128,256]{1,0:T(8,128)(2,1)} %cot_ref.1) | copy-start | bytes 196612
  23.1 4.8 %copy-start.9 = (bf16[1024,256]{1,0:T(8,128)(2,1)S(1)}, bf16[1024,256]{1,0:T(8,128)(2,1)}, u32[]{:S(2)}) copy-start(bf16[1024,256]{1,0:T(8,128)(2,1)} %wq_hbm.3) | copy-start | bytes 1572868
  23.1 4.8 %copy-start.11 = (bf16[128,256]{1,0:T(8,128)(2,1)S(1)}, bf16[128,256]{1,0:T(8,128)(2,1)}, u32[]{:S(2)}) copy-start(bf16[128,256]{1,0:T(8,128)(2,1)} %get-tuple-element.30.f_ref) | copy-start | bytes 196612
  23.1 4.8 %copy-start.14 = (bf16[128,256]{1,0:T(8,128)(2,1)S(1)}, bf16[128,256]{1,0:T(8,128)(2,1)}, u32[]{:S(2)}) copy-start(bf16[128,256]{1,0:T(8,128)(2,1)} %get-tuple-element.31.b_ref) | copy-start | bytes 196612
  23.9 4.0 %copy-start.3 = (f32[128,256]{1,0:T(8,128)S(1)}, f32[128,256]{1,0:T(8,128)}, u32[]{:S(2)}) copy-start(f32[128,256]{1,0:T(8,128)} %get-tuple-element.33.cf_ref) | copy-start | bytes 393220
  23.9 4.0 %copy-start.4 = (f32[128,256]{1,0:T(8,128)S(1)}, f32[128,256]{1,0:T(8,128)}, u32[]{:S(2)}) copy-start(f32[128,256]{1,0:T(8,128)} %get-tuple-element.34.cb_ref) | copy-start | bytes 393220
  23.9 4.0 %copy-start.5 = (bf16[128,1024]{1,0:T(8,128)(2,1)S(1)}, bf16[128,1024]{1,0:T(8,128)(2,1)}, u32[]{:S(2)}) copy-start(bf16[128,1024]{1,0:T(8,128)(2,1)} %x_hbm.5) | copy-start | bytes 786436
  23.9 12.9 %all-to-all-start.1 = ((f32[32,16,128]{2,1,0:T(8,128)}), f32[32,16,128]{2,1,0:T(8,128)S(1)}, u32[]{:S(2)}, u32[]{:S(2)}) async-start(f32[32,16,128]{2,1,0:T(8,128)} %shard_map.104), calls=%async_computation.1 | async-start | bytes 524288 | tf_op jit(solution)/shard_map/all_to_all | solution.py:345
  27.8 0.7 copy-start.31
  27.8 0.7 copy-start.33
  29.7 0.7 copy-start.21
  30.4 0.6 copy-start.27
  37.5 0.8 copy-start.6
  38.3 1.9 %copy-start.7 = (f32[128,256]{1,0:T(8,128)}, f32[128,256]{1,0:T(8,128)S(1)}, u32[]{:S(2)}) copy-start(f32[128,256]{1,0:T(8,128)S(1)} %get-tuple-element.43.dm_ref) | copy-start | bytes 393220
  40.3 0.7 copy-start.23
  41.0 0.6 copy-start.29
  41.6 15.7 %collective-permute-start = (f32[32,32,128]{2,1,0:T(8,128)}, f32[32,32,128]{2,1,0:T(8,128)S(1)}, u32[]{:S(2)}, u32[]{:S(2)}) collective-permute-start(f32[32,32,128]{2,1,0:T(8,128)} %get-tuple-element.45), channel_id=1, source_target_pairs={{0,4},{4,0},{1,5},{5,1},{2,6},{6,2},{3,7},{7,3},{8,12},{12,8},{9,1... | collective-permute-start | bytes 1572872 | tf_op jit(solution)/shard_map/ppermute | solution.py:372
  41.8 4.0 %copy-start.22 = (f32[128,512]{1,0:T(8,128)S(1)}, f32[128,512]{1,0:T(8,128)}, u32[]{:S(2)}) copy-start(f32[128,512]{1,0:T(8,128)} %copy-done.21) | copy-start | bytes 786436
  41.8 15.6 %all-to-all-start.2 = ((f32[32,32,128]{2,1,0:T(8,128)}), f32[32,32,128]{2,1,0:T(8,128)S(1)}, u32[]{:S(2)}, u32[]{:S(2)}) async-start(f32[32,32,128]{2,1,0:T(8,128)} %copy-done.6), calls=%async_computation.2 | async-start | bytes 1048576 | tf_op jit(solution)/shard_map/all_to_all | solution.py:345
  45.8 0.9 copy-start.8
  46.7 0.8 copy-start.12
  47.6 0.8 copy-start.15
  48.4 0.9 %copy-start.24 = (f32[128,512]{1,0:T(8,128)S(1)}, f32[128,512]{1,0:T(8,128)}, u32[]{:S(2)}) copy-start(f32[128,512]{1,0:T(8,128)} %copy-done.23) | copy-start | bytes 786436
  49.4 0.9 copy-start.28
  50.7 0.7 copy-start.19
  51.4 0.7 copy-start.25
  57.4 19.6 %copy-start.10 = (bf16[1024,256]{1,0:T(8,128)(2,1)S(1)}, bf16[1024,256]{1,0:T(8,128)(2,1)}, u32[]{:S(2)}) copy-start(bf16[1024,256]{1,0:T(8,128)(2,1)} %wq_hbm.3) | copy-start | bytes 1572868
  57.4 19.6 %copy-start.20 = (f32[128,512]{1,0:T(8,128)S(1)}, f32[128,512]{1,0:T(8,128)}, u32[]{:S(2)}) copy-start(f32[128,512]{1,0:T(8,128)} %copy-done.19) | copy-start | bytes 786436
  57.4 19.6 %copy-start.26 = (f32[128,256]{1,0:T(8,128)S(1)}, f32[128,256]{1,0:T(8,128)}, u32[]{:S(2)}) copy-start(f32[128,256]{1,0:T(8,128)} %copy-done.25) | copy-start | bytes 393220
  57.5 19.5 %copy-start = (bf16[1024,256]{1,0:T(8,128)(2,1)S(1)}, bf16[1024,256]{1,0:T(8,128)(2,1)}, u32[]{:S(2)}) copy-start(bf16[1024,256]{1,0:T(8,128)(2,1)} %wf_hbm.3) | copy-start | bytes 1572868
  57.5 19.5 %copy-start.1 = (bf16[1024,256]{1,0:T(8,128)(2,1)S(1)}, bf16[1024,256]{1,0:T(8,128)(2,1)}, u32[]{:S(2)}) copy-start(bf16[1024,256]{1,0:T(8,128)(2,1)} %wb_hbm.3) | copy-start | bytes 1572868
  57.5 19.5 %copy-start.2 = (bf16[1024,256]{1,0:T(8,128)(2,1)S(1)}, bf16[1024,256]{1,0:T(8,128)(2,1)}, u32[]{:S(2)}) copy-start(bf16[1024,256]{1,0:T(8,128)(2,1)} %wv_hbm.3) | copy-start | bytes 1572868
  57.5 19.5 %copy-start.13 = (bf16[128,256]{1,0:T(8,128)(2,1)S(1)}, bf16[128,256]{1,0:T(8,128)(2,1)}, u32[]{:S(2)}) copy-start(bf16[128,256]{1,0:T(8,128)(2,1)} %get-tuple-element.30.f_ref) | copy-start | bytes 196612
  57.5 19.5 %copy-start.16 = (bf16[128,256]{1,0:T(8,128)(2,1)S(1)}, bf16[128,256]{1,0:T(8,128)(2,1)}, u32[]{:S(2)}) copy-start(bf16[128,256]{1,0:T(8,128)(2,1)} %get-tuple-element.31.b_ref) | copy-start | bytes 196612
  57.5 19.5 %copy-start.18 = (bf16[128,256]{1,0:T(8,128)(2,1)S(1)}, bf16[128,256]{1,0:T(8,128)(2,1)}, u32[]{:S(2)}) copy-start(bf16[128,256]{1,0:T(8,128)(2,1)} %get-tuple-element.32.v_ref) | copy-start | bytes 196612
  57.6 19.5 %copy-start.30 = (bf16[128,256]{1,0:T(8,128)(2,1)S(1)}, bf16[128,256]{1,0:T(8,128)(2,1)}, u32[]{:S(2)}) copy-start(bf16[128,256]{1,0:T(8,128)(2,1)} %copy-done.29) | copy-start | bytes 196612
